TPU v7x, 32 devices: a whole 2x2x4 slice. The times are simulated.
32 devices in a mesh: ep: 8 (over z, x), tp: 4 (over y, core).
Axes of the slice: x: 2, y: 2, z: 4, core: 2. Of those that a mesh axis runs over, the one named last changes fastest.
Arguments:
- tokens_a: bfloat16 [2048, 2048], P('ep', 'tp'), may hold values from -60 to 60
- norm_gain_a: float32 [2048], P('tp'), may hold values from 0.1 to 1.9
- pool_weight: bfloat16 [4, 512, 512], P('tp'), may hold values from -0.25 to 0.25
- pool_scale: float32 [2048], P('tp'), may hold values from 0.1 to 1.9
- tokens_b: bfloat16 [2048, 2048], P('ep'), may hold values from -6 to 6
- norm_gain_b: float32 [2048], replicated, may hold values from 0.1 to 1.9
- routes: int32 [2048, 2], P('ep'), may hold values from 0 to 7, all different within a row; in each aligned block of 256 rows (0 to 255, 256 to 511, ...) at most 96 rows name the same one
- route_logits: float32 [2048, 2], P('ep'), may hold values from -4 to 4
- expert_gate: bfloat16 [8, 2048, 3584], P('ep', None, 'tp'), may hold values from -0.125 to 0.125
- expert_up: bfloat16 [8, 2048, 3584], P('ep', None, 'tp'), may hold values from -0.125 to 0.125
- expert_down: bfloat16 [8, 3584, 2048], P('ep', 'tp'), may hold values from -0.09375 to 0.09375
Outputs:
- mixed_a: bfloat16 [2048, 2048], P('ep', 'tp')
- moe_out: bfloat16 [2048, 2048], P('ep', 'tp')
Inputs may be any that keep to these rules, and one draw needn't show every extreme that they name: `routes`: among the 256 rows of one index of ep, at most 96 rows name any one expert, a bound that some block reaches.
All inputs are finite; a program needn't handle non-finite values.
Results may differ from a plain program's by a relative error of at most 0.012.
Values may be sent and summed in bfloat16 or wider, within the bound.
A program may use at most 128 MiB of HBM per device.

v0:
```python
import jax
import jax.numpy as jnp
from jax import lax
from jax.sharding import PartitionSpec as P

D = 2048
GROUPS = 4
TOP = 2


epsilon = 1e-06


def shifted(x, axis, by):
    peers = lax.axis_size(axis)
    pairs = [(i, i + by) for i in range(peers) if 0 <= i + by < peers]
    return lax.ppermute(x, axis, pairs)


def shards(
    tokens_a,
    norm_gain_a,
    pool_weight,
    pool_scale,
    tokens_b,
    norm_gain_b,
    routes,
    route_logits,
    expert_gate,
    expert_up,
    expert_down,
):
    tok_rows = tokens_a.shape[0]
    rows_a = tokens_a.astype(jnp.float32)
    squares = lax.psum(jnp.sum(rows_a * rows_a, axis=1), "tp")
    normed_a = (rows_a * lax.rsqrt(squares / D + epsilon)[:, None] * norm_gain_a).astype(
        jnp.bfloat16
    )
    widest = 2**GROUPS
    rim_rows = shifted(normed_a[tok_rows - (widest - 1) :], "ep", 1)
    extended = jnp.concatenate([rim_rows, normed_a], axis=0).astype(jnp.float32)
    window_len = jnp.left_shift(jnp.int32(1), lax.axis_index("tp") + 1)
    pooled = jnp.zeros((tok_rows, normed_a.shape[1]), jnp.float32)
    for offset in range(widest):
        begin_row = widest - 1 - offset
        pooled = pooled + jnp.where(
            offset < window_len, extended[begin_row : begin_row + tok_rows], 0.0
        )
    position = (
        lax.axis_index("ep") * tok_rows + jnp.arange(1, tok_rows + 1, dtype=jnp.int32)
    ).astype(jnp.float32)[:, None]
    pooled = pooled / jnp.minimum(position, window_len.astype(jnp.float32))
    difference = (pooled - normed_a.astype(jnp.float32)).astype(jnp.bfloat16)
    product = jnp.dot(difference, pool_weight[0], preferred_element_type=jnp.float32)
    mixed_a = (product * pool_scale).astype(jnp.bfloat16)
    tok_b = tokens_b.shape[0]
    width = tokens_b.shape[1]
    floats_b = tokens_b.astype(jnp.float32)
    normed_b = (
        floats_b
        * lax.rsqrt(jnp.mean(floats_b * floats_b, axis=1, keepdims=True) + epsilon)
        * norm_gain_b
    ).astype(jnp.bfloat16)
    logit_exp = jnp.exp(route_logits)
    route_weight = logit_exp / jnp.sum(logit_exp, axis=1, keepdims=True)
    n_expert = lax.axis_size("ep")
    capacity = max(2, (3 * TOP * tok_b + 2 * n_expert - 1) // (2 * n_expert))
    flat_expert = routes.reshape(-1)
    onehot = (flat_expert[:, None] == jnp.arange(n_expert, dtype=jnp.int32)[None, :]).astype(
        jnp.int32
    )
    earlier = jnp.cumsum(onehot, axis=0) - onehot
    position_in = jnp.sum(earlier * onehot, axis=1)
    slot_index = flat_expert * capacity + position_in
    token_of = jnp.arange(tok_b * TOP, dtype=jnp.int32) // TOP
    slot_token = jnp.full((n_expert * capacity,), tok_b, jnp.int32).at[slot_index].set(token_of)
    outgoing = jnp.take(normed_b, slot_token, axis=0, mode="fill", fill_value=0).reshape(
        n_expert, capacity, width
    )
    received = lax.all_to_all(outgoing, "ep", split_axis=0, concat_axis=0, tiled=True)
    item_count = received.shape[1]
    row_block = received.reshape(n_expert * item_count, width)
    gate_part = jnp.dot(row_block, expert_gate[0], preferred_element_type=jnp.float32)
    up_part = jnp.dot(row_block, expert_up[0], preferred_element_type=jnp.float32)
    hidden = (jax.nn.silu(gate_part) * up_part).astype(jnp.bfloat16)
    partial_value = jnp.dot(hidden, expert_down[0], preferred_element_type=jnp.float32).reshape(
        n_expert, item_count, width
    )
    summed = lax.psum_scatter(
        partial_value.astype(jnp.bfloat16), "tp", scatter_dimension=2, tiled=True
    ).astype(jnp.float32)
    returned_rows = lax.all_to_all(
        summed.astype(jnp.bfloat16), "ep", split_axis=0, concat_axis=0, tiled=True
    ).astype(summed.dtype)
    flat_rows = returned_rows.reshape(n_expert * capacity, returned_rows.shape[2])
    picked = jnp.take(flat_rows, slot_index, axis=0).reshape(tok_b, TOP, returned_rows.shape[2])
    combined = jnp.sum(picked * route_weight[:, :, None], axis=1)
    moe_out = combined.astype(jnp.bfloat16)
    return (mixed_a, moe_out)


def solution(mesh):
    placed = (
        P("ep", "tp"),
        P("tp"),
        P("tp", None, None),
        P("tp"),
        P("ep", None),
        P(),
        P("ep", None),
        P("ep", None),
        P("ep", None, "tp"),
        P("ep", None, "tp"),
        P("ep", "tp", None),
    )
    return jax.shard_map(
        shards,
        mesh=mesh,
        in_specs=placed,
        out_specs=(P("ep", "tp"), P("ep", "tp")),
        check_vma=False,
    )
```

profile of v0, /device:TPU:0, one launch (start us, length us, event | category | flops | bytes accessed | tf_op | source)
XLA Modules:
  0.0 187.8 jit_solution(3582748902699556048)
XLA Ops:
  7.2 0.9 copy.19
  8.1 0.1 eq.26
  8.2 0.1 reshape.111
  8.4 0.7 broadcast_multiply_fusion
  9.1 1.1 reduce-window.6
  10.2 0.2 slice_reduce_fusion
  10.5 0.1 copy.23
  10.6 0.1 mul.97
  10.9 2.4 %scatter_custom_fusion = s32[768]{0:T(1024)S(1)} fusion(s32[512]{0:T(512)S(1)} %bitcast.40, s32[512]{0:T(512)S(1)} %add_select_fusion, s32[]{:T(128)} %constant.99.clone.1), kind=kCustom, calls=%fused_computation.82 | custom fusion | bytes 3076 | tf_op jit(solution)/shard_map/scatter | solution.py:76
  13.4 1.5 fusion.9
  15.0 1.5 fusion.11
  16.5 4.3 %gather_fusion = bf16[768,2048]{1,0:T(8,128)(2,1)} fusion(bf16[256,2048]{1,0:T(8,128)(2,1)S(1)} %fusion.11, s32[1024]{0:T(1024)S(1)} %pad_clamp_fusion.1), kind=kCustom, calls=%fused_computation | custom fusion | bytes 6294528 | tf_op jit(solution)/shard_map/jit(_take)/gather | solution.py:77
  20.8 2.2 %broadcast_select_fusion = bf16[8,96,2048]{2,1,0:T(8,128)(2,1)S(1)} fusion(bf16[8,96,2048]{2,1,0:T(8,128)(2,1)} %bitcast.36, pred[8,96]{1,0:T(8,128)(4,1)S(1)} %broadcast_in_dim.59), kind=kLoop, calls=%fused_computation.10 | loop fusion | flops 1572864 | bytes 6292224 | tf_op jit(solution)/shard_map/jit(_take)/select_n | solution.py:77
  23.0 78.0 %all_to_all.10 = bf16[8,96,2048]{2,1,0:T(8,128)(2,1)S(1)} all-to-all(bf16[8,96,2048]{2,1,0:T(8,128)(2,1)S(1)} %broadcast_select_fusion), channel_id=1, replica_groups=mesh['ep'=8,'tp'=4] {'ep'}, dimensions={0} | all-to-all | bytes 6291456 | tf_op jit(solution)/shard_map/all_to_all | solution.py:80
  101.0 3.4 %fusion.2 = f32[768,896]{1,0:T(8,128)S(1)} fusion(bf16[768,2048]{1,0:T(8,128)(2,1)S(1)} %bitcast.37, bf16[1,2048,896]{2,1,0:T(8,128)(2,1)S(1)} %copy-done.5), kind=kOutput, calls=%fused_computation.5 | convolution fusion | flops 2818572288 | bytes 9568256 | tf_op jit(solution)/shard_map/dot_general | solution.py:84
  104.5 3.7 %multiply_convert_fusion = bf16[768,896]{1,0:T(8,128)(2,1)S(1)} fusion(f32[768,896]{1,0:T(8,128)S(1)} %fusion.2, bf16[768,2048]{1,0:T(8,128)(2,1)S(1)} %bitcast.38, bf16[1,2048,896]{2,1,0:T(8,128)(2,1)S(1)} %copy-done.6), kind=kOutput, calls=%fused_computation.11 | convolution fusion | flops 2822701056 | bytes 10944512 | tf_op jit(solution)/shard_map/dot_general | solution.py:83
  108.2 4.8 %fusion.6 = bf16[8,96,2048]{2,1,0:T(8,128)(2,1)} fusion(bf16[8,96,896]{2,1,0:T(8,128)(2,1)S(1)} %bitcast.42, bf16[1,896,2048]{2,1,0:T(8,128)(2,1)S(1)} %copy-done.7), kind=kOutput, calls=%fused_computation.9 | convolution fusion | flops 2820145152 | bytes 8192000 | tf_op jit(solution)/shard_map/dot_general | solution.py:86
  113.0 0.9 copy-done.1
  114.1 5.7 %psum.7 = f32[256]{0:T(256)S(1)} all-reduce(f32[256]{0:T(256)S(1)} %fusion.15), channel_id=1, replica_groups=mesh['ep'=8,'tp'=4] {'tp'}, use_global_device_ids=true, to_apply=%region_1.0 | all-reduce | flops 256 | bytes 2048 | tf_op jit(solution)/shard_map/psum | solution.py:35
  119.8 0.1 fusion.17
  119.9 3.3 %collective-permute-start = (bf16[15,512]{1,0:T(8,128)(2,1)S(1)}, bf16[15,512]{1,0:T(8,128)(2,1)S(1)}, u32[]{:S(2)}, u32[]{:S(2)}) collective-permute-start(bf16[15,512]{1,0:T(8,128)(2,1)S(1)} %slice.80), channel_id=1, source_target_pairs={{0,4},{4,8},{8,12},{12,16},{16,20},{20,24},{24,28},{1,5},{5,9},{9,... | collective-permute-start | bytes 46088 | tf_op jit(solution)/shard_map/ppermute | solution.py:17
  123.2 0.1 reduce_sum.51
  123.5 26.5 %reduce-scatter.2.cloned.1.call-done = bf16[8,96,512]{2,1,0:T(8,128)(2,1)} async-done(((bf16[8,96,2048]{2,1,0:T(8,128)(2,1)}), bf16[8,96,512]{2,1,0:T(8,128)(2,1)}) %reduce-scatter.2.cloned.1.call-update) | async-done | bytes 786448 | tf_op jit(solution)/shard_map/reduce_scatter | solution.py:89
  150.0 5.5 %all-to-all-start.1 = ((bf16[8,96,512]{2,1,0:T(8,128)(2,1)}), bf16[8,96,512]{2,1,0:T(8,128)(2,1)S(1)}, u32[]{:S(2)}, u32[]{:S(2)}) async-start(bf16[8,96,512]{2,1,0:T(8,128)(2,1)} %reduce-scatter.2.cloned.1.call-done), calls=%async_computation.2 | async-start | bytes 1572864 | tf_op jit(solution)/shard_map/all_to_all | solution.py:92
  155.6 0.2 copy.22
  155.8 0.1 copy.24
  156.0 2.0 %fusion.14 = bf16[256,512]{1,0:T(8,128)(2,1)} fusion(bf16[1,512,512]{2,1,0:T(8,128)(2,1)S(1)} %copy-done, f32[512]{0:T(512)S(1)} %copy-done.8, bf16[256,512]{1,0:T(8,128)(2,1)S(1)} %fusion.17, f32[271,512]{1,0:T(8,128)S(1)} %maximum_convert_fusion, f32[256]{0:T(256)S(1)} %convert_minimum_fusion, pred[]{:T(512)S(6)} %gt.63, pred[]{:T(512)S(6)} %gt.62, ...), kind=kOutput, calls=%fused_computation.18 | convolution fusion | flops 139067392 | bytes 9440272 | tf_op jit(solution)/shard_map/dot_general | solution.py:54
  158.0 17.5 %all-to-all-done.1 = bf16[8,96,512]{2,1,0:T(8,128)(2,1)S(1)} async-done(((bf16[8,96,512]{2,1,0:T(8,128)(2,1)}), bf16[8,96,512]{2,1,0:T(8,128)(2,1)S(1)}, u32[]{:S(2)}, u32[]{:S(2)}) %all-to-all-start.1) | async-done | bytes 786464 | tf_op jit(solution)/shard_map/all_to_all | solution.py:92
  175.6 0.3 bitcast_convert_fusion
  175.8 1.6 gather_fusion.1
  177.4 0.6 gather.15
  178.1 2.9 %multiply_reduce_fusion = bf16[256,512]{1,0:T(8,128)(2,1)} fusion(f32[256,2,512]{2,1,0:T(2,128)S(1)} %gather.15, pred[256,2]{1,0:T(8,128)(4,1)S(1)} %copy.22, f32[256,2]{1,0:T(8,128)S(1)} %copy.24), kind=kLoop, calls=%fused_computation.19 | loop fusion | flops 655360 | bytes 1313280 | tf_op jit(solution)/shard_map/reduce_sum | solution.py:97
  (41 shorter events, 0.7 us)
Async XLA Ops:
  7.2 148.8 %copy-start = (bf16[1,512,512]{2,1,0:T(8,128)(2,1)S(1)}, bf16[1,512,512]{2,1,0:T(8,128)(2,1)}, u32[]{:S(2)}) copy-start(bf16[1,512,512]{2,1,0:T(8,128)(2,1)} %param.13) | copy-start | bytes 1572868
  7.2 142.8 %reduce-scatter.2.cloned.1.call-start = ((), (), s32[]{:S(2)}) async-start(), calls=%async_computation.3 | async-start | bytes 3932160 | tf_op jit(solution)/shard_map/reduce_scatter | solution.py:89
  23.0 78.1 %copy-start.5 = (bf16[1,2048,896]{2,1,0:T(8,128)(2,1)S(1)}, bf16[1,2048,896]{2,1,0:T(8,128)(2,1)}, u32[]{:S(2)}) copy-start(bf16[1,2048,896]{2,1,0:T(8,128)(2,1)} %param.20) | copy-start | bytes 11010052
  101.0 3.4 %copy-start.6 = (bf16[1,2048,896]{2,1,0:T(8,128)(2,1)S(1)}, bf16[1,2048,896]{2,1,0:T(8,128)(2,1)}, u32[]{:S(2)}) copy-start(bf16[1,2048,896]{2,1,0:T(8,128)(2,1)} %param.19) | copy-start | bytes 11010052
  104.5 3.7 %copy-start.7 = (bf16[1,896,2048]{2,1,0:T(8,128)(2,1)S(1)}, bf16[1,896,2048]{2,1,0:T(8,128)(2,1)}, u32[]{:S(2)}) copy-start(bf16[1,896,2048]{2,1,0:T(8,128)(2,1)} %param.21) | copy-start | bytes 11010052
  113.0 0.9 copy-start.1
  113.0 6.8 %copy-start.4 = (f32[512]{0:T(512)S(1)}, f32[512]{0:T(512)}, u32[]{:S(2)}) copy-start(f32[512]{0:T(512)} %param.12) | copy-start | bytes 6148
  113.0 10.5 %copy-start.3 = (f32[256,2]{0,1:T(2,128)S(1)}, f32[256,2]{0,1:T(2,128)}, u32[]{:S(2)}) copy-start(f32[256,2]{0,1:T(2,128)} %param.18) | copy-start | bytes 6148
  113.0 42.5 %copy-start.2 = (s32[256,2]{0,1:T(2,128)S(1)}, s32[256,2]{0,1:T(2,128)}, u32[]{:S(2)}) copy-start(s32[256,2]{0,1:T(2,128)} %param.17) | copy-start | bytes 6148
  113.0 43.0 %copy-start.8 = (f32[512]{0:T(512)S(1)}, f32[512]{0:T(512)}, u32[]{:S(2)}) copy-start(f32[512]{0:T(512)} %param.14) | copy-start | bytes 6148
  119.9 36.0 %collective-permute-start = (bf16[15,512]{1,0:T(8,128)(2,1)S(1)}, bf16[15,512]{1,0:T(8,128)(2,1)S(1)}, u32[]{:S(2)}, u32[]{:S(2)}) collective-permute-start(bf16[15,512]{1,0:T(8,128)(2,1)S(1)} %slice.80), channel_id=1, source_target_pairs={{0,4},{4,8},{8,12},{12,16},{16,20},{20,24},{24,28},{1,5},{5,9},{9,... | collective-permute-start | bytes 46088 | tf_op jit(solution)/shard_map/ppermute | solution.py:17
  150.0 25.6 %all-to-all-start.1 = ((bf16[8,96,512]{2,1,0:T(8,128)(2,1)}), bf16[8,96,512]{2,1,0:T(8,128)(2,1)S(1)}, u32[]{:S(2)}, u32[]{:S(2)}) async-start(bf16[8,96,512]{2,1,0:T(8,128)(2,1)} %reduce-scatter.2.cloned.1.call-done), calls=%async_computation.2 | async-start | bytes 1572864 | tf_op jit(solution)/shard_map/all_to_all | solution.py:92
Sparse Core Ops, SparseCore 0:
  113.2 36.7 reduce-scatter.1
where the time goes:
time: 188 us
  blocking collectives  83.7 us (45%)
  waiting for transfers between devices  44 us (23%)
  between operations  14.4 us (8%)
  matrix products  13.9 us (7%)
  local copies, waits for them, and re-layouts  12.2 us (6%)
  other arithmetic  10.7 us (6%)
  starting transfers between devices  8.86 us (5%)
    all_to_all x1, blocking collectives, shards(): lax.all_to_all(outgoing, 'ep', split_axis=0, concat_axis=0, tiled=True)  78 us
    reduce_scatter x1, waiting for transfers between devices, shards(): lax.psum_scatter(partial_value.astype(jnp.bfloat16), 'tp', scatter_dimens...  26.5 us
    all_to_all x1, waiting for transfers between devices, shards(): lax.all_to_all(summed.astype(jnp.bfloat16), 'ep', split_axis=0, concat_ax...  17.5 us
    psum x1, blocking collectives, shards(): squares = lax.psum(jnp.sum(rows_a * rows_a, axis=1), 'tp')  5.66 us
    all_to_all x1, starting transfers between devices, shards(): lax.all_to_all(summed.astype(jnp.bfloat16), 'ep', split_axis=0, concat_ax...  5.5 us
    dot_general x1, matrix products, shards(): jnp.dot(hidden, expert_down[0], preferred_element_type=jnp.float32)  4.81 us
    gather x1, local copies, waits for them, and re-layouts, shards(): jnp.take(normed_b, slot_token, axis=0, mode='fill', fill_value=0)  4.27 us
  transfers between devices with their start and end apart: 3, of which 2 were waited for; matrix products, arithmetic and copies ran while one was open for 2% of the time, Pallas kernels for 0%

commit v1 on v0

v1 whole, which is shorter than its diff:
```python
import functools

import jax
import jax.numpy as jnp
from jax import lax
from jax.experimental import pallas as pl
from jax.experimental.pallas import tpu as pltpu
from jax.sharding import PartitionSpec as P

GROUPS = 4
TOP = 2
MESH = pl.DeviceIdType.MESH
F32 = jnp.float32
BF16 = jnp.bfloat16

epsilon = 1e-06


def dot(a, b):
    return jnp.dot(a, b, preferred_element_type=F32)


def body(
    n,
    cap,
    group,
    ta_ref,
    ga_ref,
    pw_ref,
    ps_ref,
    tb_ref,
    gb_ref,
    rt_ref,
    rc_ref,
    rl_ref,
    wg_hbm,
    wu_hbm,
    wd_hbm,
    mixed_ref,
    moe_ref,
    wg,
    wu,
    wd,
    nb,
    outgoing,
    rows,
    part,
    core_in,
    y_out,
    y_in,
    back_out,
    back_in,
    sq,
    rim_out,
    rim_in,
    w_sem,
    send,
    recv,
    sq_send,
    sq_recv,
    rim_send,
    rim_recv,
):
    ep = lax.axis_index("ep")
    tp = lax.axis_index("tp")
    core = lax.rem(tp, 2)
    y = lax.div(tp, 2)
    core_peer = tp + 1 - 2 * core
    y_peer = lax.rem(tp + 2, 4)
    cross_peer = lax.rem(core_peer + 2, 4)
    tok, quarter = ta_ref.shape
    groups = n // group

    barrier = pltpu.get_barrier_semaphore()

    def greet(k, _):
        pl.semaphore_signal(
            barrier,
            inc=1,
            device_id={"ep": lax.rem(ep + k, n), "tp": tp},
            device_id_type=MESH,
        )
        return 0

    lax.fori_loop(1, n, greet, 0)
    for peer in (core_peer, y_peer, cross_peer):
        pl.semaphore_signal(
            barrier, inc=1, device_id={"ep": ep, "tp": peer}, device_id_type=MESH
        )
    weights = [
        pltpu.make_async_copy(src.at[0], dst, w_sem.at[i])
        for i, (src, dst) in enumerate(((wg_hbm, wg), (wu_hbm, wu), (wd_hbm, wd)))
    ]
    for copy in weights:
        copy.start()

    def offset_of(j):
        half = lax.div(j + 1, 2)
        return jnp.where(lax.rem(j, 2) == 1, half, lax.rem(n - half, n))

    def remote(kind, j, src, dst, peer_ep, peer_tp):
        return pltpu.make_async_remote_copy(
            src_ref=src,
            dst_ref=dst,
            send_sem=send.at[kind, j],
            recv_sem=recv.at[kind, j],
            device_id={"ep": peer_ep, "tp": peer_tp},
            device_id_type=MESH,
        )

    def columns(index):
        return pl.ds(pl.multiple_of(index * quarter, quarter), quarter)

    def dispatch(j):
        return remote(
            0,
            j,
            outgoing.at[j],
            rows.at[j, :, columns(tp)],
            lax.rem(ep + offset_of(j), n),
            tp,
        )

    def to_core(j):
        view = rows.at[j, :, columns(tp)]
        return remote(1, j, view, view, ep, core_peer)

    def to_y(j):
        view = rows.at[j, :, columns(tp)]
        return remote(2, j, view, view, ep, y_peer)

    def relay(j):
        view = rows.at[j, :, columns(y_peer)]
        return remote(3, j, view, view, ep, core_peer)

    def part_core(j):
        return remote(4, j, part.at[1 - core, j], core_in.at[j], ep, core_peer)

    def part_y(j):
        return remote(5, j, y_out.at[j], y_in.at[j], ep, y_peer)

    def give_back(j):
        return remote(
            6,
            j,
            back_out.at[j],
            back_in.at[j],
            lax.rem(ep - offset_of(j) + n, n),
            tp,
        )

    rows_a = ta_ref[...].astype(F32)
    own_sq = jnp.sum(rows_a * rows_a, axis=1, keepdims=True)
    sq[0] = jnp.transpose(jnp.broadcast_to(own_sq, (tok, 128)))[:8]

    floats_b = tb_ref[...].astype(F32)
    scale_b = lax.rsqrt(
        jnp.mean(floats_b * floats_b, axis=1, keepdims=True) + epsilon
    )
    nb[...] = (floats_b * scale_b * gb_ref[...]).astype(BF16)

    def slot_of(expert, place):
        k = expert - ep
        k = jnp.where(k < 0, k + n, k)
        j = jnp.where(k == 0, 0, jnp.where(2 * k <= n, 2 * k - 1, 2 * (n - k)))
        return j * cap + place

    def slots(axis):
        shape = (n, tok) if axis == 0 else (tok, n)
        ref = rt_ref if axis == 0 else rc_ref
        experts = [
            ref[k : k + 1, :] if axis == 0 else ref[:, k : k + 1] for k in range(TOP)
        ]
        index = lax.broadcasted_iota(jnp.int32, shape, axis)
        hot = [(index == e).astype(F32) for e in experts]
        before = (
            lax.broadcasted_iota(jnp.int32, (tok, tok), axis)
            < lax.broadcasted_iota(jnp.int32, (tok, tok), 1 - axis)
        ).astype(F32).astype(BF16)
        total = (hot[0] + hot[1]).astype(BF16)
        earlier = dot(total, before) if axis == 0 else dot(before, total)
        return [
            slot_of(
                e, jnp.sum(earlier * h, axis=axis, keepdims=True).astype(jnp.int32)
            )
            for e, h in zip(experts, hot)
        ]

    lane_slots = slots(0)
    chosen = lax.broadcasted_iota(jnp.int32, (n * cap, tok), 0)
    hot = (
        ((chosen == lane_slots[0]) | (chosen == lane_slots[1]))
        .astype(F32)
        .astype(BF16)
    )
    outgoing[...] = (
        dot(hot, nb[:, columns(tp)]).astype(BF16).reshape(n, cap, quarter)
    )

    pl.semaphore_wait(barrier, n + 2)
    sq_copies = [
        pltpu.make_async_remote_copy(
            src_ref=sq.at[0],
            dst_ref=sq.at[i],
            send_sem=sq_send.at[i - 1],
            recv_sem=sq_recv.at[i - 1],
            device_id={"ep": ep, "tp": peer},
            device_id_type=MESH,
        )
        for i, peer in ((1, core_peer), (2, y_peer), (3, cross_peer))
    ]
    for copy in sq_copies:
        copy.start()

    def start_dispatch(j, _):
        dispatch(j).start()
        return 0

    lax.fori_loop(1, n, start_dispatch, 0)
    rows[0] = dot(hot[:cap], nb[...]).astype(BF16)

    for copy in sq_copies:
        copy.wait_recv()
    total_sq = (sq[0] + sq[1]) + (sq[2] + sq[3])
    squares = jnp.transpose(jnp.broadcast_to(total_sq[:1], (128, tok)))[:, :1]
    width = quarter * 4
    normed_a = (rows_a * lax.rsqrt(squares / width + epsilon) * ga_ref[...]).astype(
        BF16
    )
    widest = 2**GROUPS
    rim_out[...] = normed_a[tok - widest :]
    rim = pltpu.make_async_remote_copy(
        src_ref=rim_out,
        dst_ref=rim_in,
        send_sem=rim_send,
        recv_sem=rim_recv,
        device_id={"ep": lax.rem(ep + 1, n), "tp": tp},
        device_id_type=MESH,
    )
    rim.start()

    def forward(g):
        def step(j, _):
            @pl.when(j > 0)
            def _():
                dispatch(j).wait_recv()
                to_core(j).start()
                to_y(j).start()

            return 0

        lax.fori_loop(g * group, (g + 1) * group, step, 0)

    forward(0)

    rim.wait_recv()
    before_own = jnp.where(ep == 0, 0.0, rim_in[...].astype(F32))
    own = normed_a.astype(F32)
    pooled = jnp.concatenate([before_own, own], axis=0)
    wanted = None
    for level in range(GROUPS):
        pooled = pooled + pltpu.roll(pooled, 2**level, 0)
        wanted = pooled if wanted is None else jnp.where(tp >= level, pooled, wanted)
    window_len = jnp.left_shift(jnp.int32(1), tp + 1)
    position = ep * tok + 1 + lax.broadcasted_iota(jnp.int32, (tok, 1), 0)
    divisor = jnp.minimum(position, window_len).astype(F32)
    difference = (wanted[widest:] / divisor - own).astype(BF16)
    mixed_ref[...] = (dot(difference, pw_ref[0]) * ps_ref[...]).astype(BF16)

    for copy in weights:
        copy.wait()

    def sum_y(j, _):
        part_core(j).wait_recv()
        away = columns(1 - y)
        y_out[j] = (
            part[core, j, :, away].astype(F32) + core_in[j, :, away].astype(F32)
        ).astype(BF16)
        part_y(j).start()
        return 0

    def sum_all(j, _):
        part_y(j).wait_recv()
        here = columns(y)
        value = (
            part[core, j, :, here].astype(F32)
            + core_in[j, :, here].astype(F32)
            + y_in[j].astype(F32)
        ).astype(BF16)

        @pl.when(j > 0)
        def _():
            back_out[j] = value
            give_back(j).start()

        @pl.when(j == 0)
        def _():
            back_in[j] = value

        return 0

    def compute(g, _):
        first, last = g * group, (g + 1) * group

        def pass_on(j, _):
            @pl.when(j > 0)
            def _():
                to_y(j).wait_recv()
                relay(j).start()

            return 0

        def arrived(j, _):
            @pl.when(j > 0)
            def _():
                to_core(j).wait_recv()
                relay(j).wait_recv()

            return 0

        lax.fori_loop(first, last, pass_on, 0)
        lax.fori_loop(first, last, arrived, 0)
        block = rows[pl.ds(first, group)].reshape(group * cap, width)
        gate = dot(block, wg[...])
        up = dot(block, wu[...])
        hidden = (gate / (1.0 + jnp.exp(-gate)) * up).astype(BF16)
        for q in range(4):
            piece = dot(hidden, wd[:, q * quarter : (q + 1) * quarter]).astype(BF16)
            half = (q // 2) * quarter
            part[q % 2, pl.ds(first, group), :, half : half + quarter] = piece.reshape(
                group, cap, quarter
            )

        def start_part(j, _):
            part_core(j).start()
            return 0

        lax.fori_loop(first, last, start_part, 0)

        @pl.when(g + 1 < groups)
        def _():
            forward(g + 1)

        lax.fori_loop(first, last, sum_y, 0)

        @pl.when(g > 0)
        def _():
            lax.fori_loop(first - group, last - group, sum_all, 0)

        return 0

    lax.fori_loop(0, groups, compute, 0)
    lax.fori_loop(n - group, n, sum_all, 0)

    def finish(j, _):
        part_core(j).wait_send()
        part_y(j).wait_send()

        @pl.when(j > 0)
        def _():
            dispatch(j).wait_send()
            to_core(j).wait_send()
            to_y(j).wait_send()
            relay(j).wait_send()
            give_back(j).wait_send()
            give_back(j).wait_recv()

        return 0

    weight_exp = jnp.exp(rl_ref[...])
    route_weight = weight_exp / jnp.sum(weight_exp, axis=1, keepdims=True)
    chosen = lax.broadcasted_iota(jnp.int32, (tok, n * cap), 1)
    picks = [(chosen == s).astype(F32).astype(BF16) for s in slots(1)]
    for copy in sq_copies:
        copy.wait_send()
    rim.wait_send()
    lax.fori_loop(0, n, finish, 0)
    flat = back_in[...].reshape(n * cap, quarter)
    combined = jnp.zeros((tok, quarter), F32)
    for k in range(TOP):
        combined = combined + dot(picks[k], flat) * route_weight[:, k : k + 1]
    moe_ref[...] = combined.astype(BF16)


def shards(
    n,
    tokens_a,
    norm_gain_a,
    pool_weight,
    pool_scale,
    tokens_b,
    norm_gain_b,
    routes,
    route_logits,
    expert_gate,
    expert_up,
    expert_down,
):
    tok, width = tokens_b.shape
    quarter = tokens_a.shape[1]
    hidden = expert_gate.shape[2]
    most = max(2, (3 * TOP * tok + 2 * n - 1) // (2 * n))
    cap = -(-most // 16) * 16
    group = 1
    while n % (2 * group) == 0 and 2 * group * cap <= 256:
        group = 2 * group
    vmem = pl.BlockSpec(memory_space=pltpu.VMEM)
    hbm = pl.BlockSpec(memory_space=pl.ANY)
    slab = pltpu.VMEM((n, cap, quarter), BF16)
    dma = pltpu.SemaphoreType.DMA
    return pl.pallas_call(
        functools.partial(body, n, cap, group),
        out_shape=(
            jax.ShapeDtypeStruct((tok, quarter), BF16),
            jax.ShapeDtypeStruct((tok, quarter), BF16),
        ),
        in_specs=[vmem] * 9 + [hbm] * 3,
        out_specs=(vmem, vmem),
        scratch_shapes=[
            pltpu.VMEM((width, hidden), BF16),
            pltpu.VMEM((width, hidden), BF16),
            pltpu.VMEM((hidden, width), BF16),
            pltpu.VMEM((tok, width), BF16),
            slab,
            pltpu.VMEM((n, cap, width), BF16),
            pltpu.VMEM((2, n, cap, 2 * quarter), BF16),
            pltpu.VMEM((n, cap, 2 * quarter), BF16),
            slab,
            slab,
            slab,
            slab,
            pltpu.VMEM((4, 8, tok), F32),
            pltpu.VMEM((2**GROUPS, quarter), BF16),
            pltpu.VMEM((2**GROUPS, quarter), BF16),
            dma((3,)),
            dma((7, n)),
            dma((7, n)),
            dma((3,)),
            dma((3,)),
            dma,
            dma,
        ],
        compiler_params=pltpu.CompilerParams(
            collective_id=0,
            has_side_effects=True,
            vmem_limit_bytes=60 * 1024 * 1024,
        ),
    )(
        tokens_a,
        norm_gain_a[None, :],
        pool_weight,
        pool_scale[None, :],
        tokens_b,
        norm_gain_b[None, :],
        routes.T,
        routes,
        route_logits,
        expert_gate,
        expert_up,
        expert_down,
    )


def solution(mesh):
    placed = (
        P("ep", "tp"),
        P("tp"),
        P("tp", None, None),
        P("tp"),
        P("ep", None),
        P(),
        P("ep", None),
        P("ep", None),
        P("ep", None, "tp"),
        P("ep", None, "tp"),
        P("ep", "tp", None),
    )
    return jax.shard_map(
        functools.partial(shards, mesh.shape["ep"]),
        mesh=mesh,
        in_specs=placed,
        out_specs=(P("ep", "tp"), P("ep", "tp")),
        check_vma=False,
    )
```

time: 188 us -> 81.3 us (0.43)
  blocking collectives: 83.7 us -> 0 us
  Pallas kernels: 0 us -> 74.1 us
  waiting for transfers between devices: 44 us -> 0 us
  matrix products: 13.9 us -> 0 us
  between operations: 14.4 us -> 0.64 us
  other arithmetic: 10.7 us -> 0 us
  starting transfers between devices: 8.86 us -> 0 us
  local copies, waits for them, and re-layouts: 12.2 us -> 6.29 us
    all_to_all x1 -> x0, blocking collectives: 78 us -> none  [shards(): lax.all_to_all(outgoing, 'ep', split_axis=0, concat_axis=0, tiled=True)]
    pallas_call x0 -> x1, Pallas kernels: none -> 74.1 us  [shards(): pl.pallas_call(functools.partial(body, n, cap, group), out_shape=(jax.Sha...]
    reduce_scatter x1 -> x0, waiting for transfers between devices: 26.5 us -> none  [shards(): lax.psum_scatter(partial_value.astype(jnp.bfloat16), 'tp', scatter_dimens...]
    all_to_all x1 -> x0, waiting for transfers between devices: 17.5 us -> none  [shards(): lax.all_to_all(summed.astype(jnp.bfloat16), 'ep', split_axis=0, concat_ax...]
    dot_general x4 -> x0, matrix products: 13.9 us -> none  [the longest x1 4.81 us: shards(): jnp.dot(hidden, expert_down[0], preferred_element_type=jnp.float32)]
    gather x3 -> x0, local copies, waits for them, and re-layouts: 6.51 us -> none  [the longest x1 4.27 us: shards(): jnp.take(normed_b, slot_token, axis=0, mode='fill', fill_value=0)]
    psum x1 -> x0, blocking collectives: 5.66 us -> none  [shards(): squares = lax.psum(jnp.sum(rows_a * rows_a, axis=1), 'tp')]
    all_to_all x1 -> x0, starting transfers between devices: 5.5 us -> none  [shards(): lax.all_to_all(summed.astype(jnp.bfloat16), 'ep', split_axis=0, concat_ax...]
  transfers between devices with their start and end apart: 3 -> 0, of which waited for: 2 -> 0; matrix products, arithmetic and copies ran while one was open for 2% -> 0% of each run, Pallas kernels for 0% -> 0%
where the time goes in v1:
time: 81.3 us; the launch traced here: 81 us
  Pallas kernels  74.1 us (91%)
  local copies, waits for them, and re-layouts  6.29 us (8%)
    pallas_call x1, Pallas kernels, shards(): pl.pallas_call(functools.partial(body, n, cap, group), out_shape=(jax.Sha...  74.1 us
    unnamed x4, local copies, waits for them, and re-layouts  6.29 us

profile of v1, /device:TPU:0, one launch (start us, length us, event | category | flops | bytes accessed | tf_op | source)
XLA Modules:
  0.0 81.0 jit_solution(10952374985762065744)
XLA Ops:
  0.6 1.5 %copy.14.rl_ref = f32[256,2]{1,0:T(8,128)} copy(f32[256,2]{0,1:T(2,128)} %param.18) | data formatting | bytes 4096 | tf_op args[7]
  2.1 1.5 %copy.13.rc_ref = s32[256,2]{1,0:T(8,128)} copy(s32[256,2]{0,1:T(2,128)} %param.17) | data formatting | bytes 4096 | tf_op args[6]
  3.6 74.1 %shard_map.122 = (bf16[256,512]{1,0:T(8,128)(2,1)}, bf16[256,512]{1,0:T(8,128)(2,1)}) custom-call(bf16[256,512]{1,0:T(8,128)(2,1)} %ta_ref.1, f32[1,512]{1,0:T(1,128)} %bitcast.6, bf16[1,512,512]{2,1,0:T(8,128)(2,1)} %pw_ref.1, f32[1,512]{1,0:T(1,128)} %bitcast.7, bf16[256,2048]{1,0:T(8,128)(2,1)} %tb_ref.1, f32[1,2048]{1,0:T(1,128)} %bitcast.5, ...), custom_call_target="tpu_custom_call" | custom-call | tf_op jit(solution)/shard_map/pallas_call | solution.py:411
  77.7 1.7 %copy.17 = bf16[256,512]{1,0:T(8,128)(2,1)} copy(bf16[256,512]{1,0:T(8,128)(2,1)} %get-tuple-element.4) | data formatting | bytes 524288
  79.4 1.7 %copy.18 = bf16[256,512]{1,0:T(8,128)(2,1)} copy(bf16[256,512]{1,0:T(8,128)(2,1)} %get-tuple-element.5) | data formatting | bytes 524288

commit v2 on v1

--- a/solution.py
+++ b/solution.py
@@ -31,13 +31,11 @@
     tb_ref,
     gb_ref,
     rt_ref,
-    rc_ref,
     rl_ref,
     wg_hbm,
     wu_hbm,
     wd_hbm,
-    mixed_ref,
-    moe_ref,
+    both_ref,
     wg,
     wu,
     wd,
@@ -121,23 +119,47 @@
             tp,
         )
 
-    def to_core(j):
-        view = rows.at[j, :, columns(tp)]
-        return remote(1, j, view, view, ep, core_peer)
-
-    def to_y(j):
-        view = rows.at[j, :, columns(tp)]
-        return remote(2, j, view, view, ep, y_peer)
-
-    def relay(j):
-        view = rows.at[j, :, columns(y_peer)]
-        return remote(3, j, view, view, ep, core_peer)
-
-    def part_core(j):
-        return remote(4, j, part.at[1 - core, j], core_in.at[j], ep, core_peer)
-
-    def part_y(j):
-        return remote(5, j, y_out.at[j], y_in.at[j], ep, y_peer)
+    def span(g):
+        if isinstance(g, int) and g == 0:
+            return pl.ds(1, group - 1)
+        return pl.ds(g * group, group)
+
+    def to_core(g):
+        view = rows.at[span(g), :, columns(tp)]
+        return remote(1, g, view, view, ep, core_peer)
+
+    def to_y(g):
+        view = rows.at[span(g), :, columns(tp)]
+        return remote(2, g, view, view, ep, y_peer)
+
+    def relay(g):
+        view = rows.at[span(g), :, columns(y_peer)]
+        return remote(3, g, view, view, ep, core_peer)
+
+    def part_core(g):
+        many = pl.ds(g * group, group)
+        return remote(
+            4, g, part.at[1 - core, many], core_in.at[many], ep, core_peer
+        )
+
+    def part_y(g):
+        many = pl.ds(g * group, group)
+        return remote(5, g, y_out.at[many], y_in.at[many], ep, y_peer)
+
+    def each(g, act):
+        if isinstance(g, int):
+            if g > 0 or group > 1:
+                act(g)
+            return
+        if group > 1:
+
+            @pl.when(g == 0)
+            def _():
+                act(0)
+
+        @pl.when(g > 0)
+        def _():
+            act(g)
 
     def give_back(j):
         return remote(
@@ -165,28 +187,22 @@
         j = jnp.where(k == 0, 0, jnp.where(2 * k <= n, 2 * k - 1, 2 * (n - k)))
         return j * cap + place
 
-    def slots(axis):
-        shape = (n, tok) if axis == 0 else (tok, n)
-        ref = rt_ref if axis == 0 else rc_ref
-        experts = [
-            ref[k : k + 1, :] if axis == 0 else ref[:, k : k + 1] for k in range(TOP)
-        ]
-        index = lax.broadcasted_iota(jnp.int32, shape, axis)
-        hot = [(index == e).astype(F32) for e in experts]
-        before = (
-            lax.broadcasted_iota(jnp.int32, (tok, tok), axis)
-            < lax.broadcasted_iota(jnp.int32, (tok, tok), 1 - axis)
-        ).astype(F32).astype(BF16)
-        total = (hot[0] + hot[1]).astype(BF16)
-        earlier = dot(total, before) if axis == 0 else dot(before, total)
-        return [
-            slot_of(
-                e, jnp.sum(earlier * h, axis=axis, keepdims=True).astype(jnp.int32)
-            )
-            for e, h in zip(experts, hot)
-        ]
-
-    lane_slots = slots(0)
+    experts = [rt_ref[k : k + 1, :] for k in range(TOP)]
+    index = lax.broadcasted_iota(jnp.int32, (n, tok), 0)
+    named = [(index == e).astype(F32) for e in experts]
+    before = (
+        (
+            lax.broadcasted_iota(jnp.int32, (tok, tok), 0)
+            < lax.broadcasted_iota(jnp.int32, (tok, tok), 1)
+        )
+        .astype(F32)
+        .astype(BF16)
+    )
+    earlier = dot((named[0] + named[1]).astype(BF16), before)
+    lane_slots = [
+        slot_of(e, jnp.sum(earlier * h, axis=0, keepdims=True).astype(jnp.int32))
+        for e, h in zip(experts, named)
+    ]
     chosen = lax.broadcasted_iota(jnp.int32, (n * cap, tok), 0)
     hot = (
         ((chosen == lane_slots[0]) | (chosen == lane_slots[1]))
@@ -244,12 +260,16 @@
             @pl.when(j > 0)
             def _():
                 dispatch(j).wait_recv()
-                to_core(j).start()
-                to_y(j).start()
 
             return 0
 
         lax.fori_loop(g * group, (g + 1) * group, step, 0)
+
+        def act(g):
+            to_y(g).start()
+            to_core(g).start()
+
+        each(g, act)
 
     forward(0)
 
@@ -265,61 +285,56 @@
     position = ep * tok + 1 + lax.broadcasted_iota(jnp.int32, (tok, 1), 0)
     divisor = jnp.minimum(position, window_len).astype(F32)
     difference = (wanted[widest:] / divisor - own).astype(BF16)
-    mixed_ref[...] = (dot(difference, pw_ref[0]) * ps_ref[...]).astype(BF16)
+    both_ref[0] = dot(difference, pw_ref[0]) * ps_ref[...]
 
     for copy in weights:
         copy.wait()
 
-    def sum_y(j, _):
-        part_core(j).wait_recv()
-        away = columns(1 - y)
-        y_out[j] = (
-            part[core, j, :, away].astype(F32) + core_in[j, :, away].astype(F32)
+    def sum_y(g):
+        part_core(g).wait_recv()
+        away, many = columns(1 - y), pl.ds(g * group, group)
+        y_out[many] = (
+            part[core, many, :, away].astype(F32) + core_in[many, :, away].astype(F32)
         ).astype(BF16)
-        part_y(j).start()
-        return 0
-
-    def sum_all(j, _):
-        part_y(j).wait_recv()
+        part_y(g).start()
+
+    def sum_all(g):
+        part_y(g).wait_recv()
         here = columns(y)
-        value = (
-            part[core, j, :, here].astype(F32)
-            + core_in[j, :, here].astype(F32)
-            + y_in[j].astype(F32)
-        ).astype(BF16)
-
-        @pl.when(j > 0)
-        def _():
-            back_out[j] = value
-            give_back(j).start()
-
-        @pl.when(j == 0)
-        def _():
-            back_in[j] = value
-
-        return 0
-
-    def compute(g, _):
-        first, last = g * group, (g + 1) * group
-
-        def pass_on(j, _):
+
+        def step(j, _):
+            value = (
+                part[core, j, :, here].astype(F32)
+                + core_in[j, :, here].astype(F32)
+                + y_in[j].astype(F32)
+            ).astype(BF16)
+
             @pl.when(j > 0)
             def _():
-                to_y(j).wait_recv()
-                relay(j).start()
+                back_out[j] = value
+                give_back(j).start()
+
+            @pl.when(j == 0)
+            def _():
+                back_in[j] = value
 
             return 0
 
-        def arrived(j, _):
-            @pl.when(j > 0)
-            def _():
-                to_core(j).wait_recv()
-                relay(j).wait_recv()
-
-            return 0
-
-        lax.fori_loop(first, last, pass_on, 0)
-        lax.fori_loop(first, last, arrived, 0)
+        lax.fori_loop(g * group, (g + 1) * group, step, 0)
+
+    def compute(g, _):
+        first = g * group
+
+        def pass_on(g):
+            to_y(g).wait_recv()
+            relay(g).start()
+
+        def arrived(g):
+            to_core(g).wait_recv()
+            relay(g).wait_recv()
+
+        each(g, pass_on)
+        each(g, arrived)
         block = rows[pl.ds(first, group)].reshape(group * cap, width)
         gate = dot(block, wg[...])
         up = dot(block, wu[...])
@@ -331,55 +346,72 @@
                 group, cap, quarter
             )
 
-        def start_part(j, _):
-            part_core(j).start()
-            return 0
-
-        lax.fori_loop(first, last, start_part, 0)
-
-        @pl.when(g + 1 < groups)
+        part_core(g).start()
+
+        @pl.when(g + 2 < groups)
         def _():
-            forward(g + 1)
-
-        lax.fori_loop(first, last, sum_y, 0)
-
-        @pl.when(g > 0)
+            forward(g + 2)
+
+        sum_y(g)
+
+        @pl.when(g > 1)
         def _():
-            lax.fori_loop(first - group, last - group, sum_all, 0)
+            sum_all(g - 2)
 
         return 0
 
+    if groups > 1:
+        forward(1)
     lax.fori_loop(0, groups, compute, 0)
-    lax.fori_loop(n - group, n, sum_all, 0)
+    for g in range(max(0, groups - 2), groups):
+        sum_all(g)
 
     def finish(j, _):
-        part_core(j).wait_send()
-        part_y(j).wait_send()
-
         @pl.when(j > 0)
         def _():
             dispatch(j).wait_send()
-            to_core(j).wait_send()
-            to_y(j).wait_send()
-            relay(j).wait_send()
             give_back(j).wait_send()
             give_back(j).wait_recv()
 
         return 0
 
+    def sent(g, _):
+        part_core(g).wait_send()
+        part_y(g).wait_send()
+
+        def act(g):
+            to_core(g).wait_send()
+            to_y(g).wait_send()
+            relay(g).wait_send()
+
+        each(g, act)
+        return 0
+
     weight_exp = jnp.exp(rl_ref[...])
-    route_weight = weight_exp / jnp.sum(weight_exp, axis=1, keepdims=True)
+    route_weight = weight_exp / jnp.sum(weight_exp, axis=0, keepdims=True)
+    line = lax.broadcasted_iota(jnp.int32, (128, tok), 0)
+    stacked = jnp.zeros((128, tok), F32)
+    for i, row in enumerate(
+        [s.astype(F32) for s in lane_slots]
+        + [route_weight[k : k + 1, :] for k in range(TOP)]
+    ):
+        stacked = jnp.where(line == i, row, stacked)
+    turned = jnp.transpose(stacked)
     chosen = lax.broadcasted_iota(jnp.int32, (tok, n * cap), 1)
-    picks = [(chosen == s).astype(F32).astype(BF16) for s in slots(1)]
+    picks = [
+        (chosen == turned[:, k : k + 1].astype(jnp.int32)).astype(F32).astype(BF16)
+        for k in range(TOP)
+    ]
     for copy in sq_copies:
         copy.wait_send()
     rim.wait_send()
+    lax.fori_loop(0, groups, sent, 0)
     lax.fori_loop(0, n, finish, 0)
     flat = back_in[...].reshape(n * cap, quarter)
     combined = jnp.zeros((tok, quarter), F32)
     for k in range(TOP):
-        combined = combined + dot(picks[k], flat) * route_weight[:, k : k + 1]
-    moe_ref[...] = combined.astype(BF16)
+        combined = combined + dot(picks[k], flat) * turned[:, TOP + k : TOP + k + 1]
+    both_ref[1] = combined
 
 
 def shards(
@@ -408,14 +440,11 @@
     hbm = pl.BlockSpec(memory_space=pl.ANY)
     slab = pltpu.VMEM((n, cap, quarter), BF16)
     dma = pltpu.SemaphoreType.DMA
-    return pl.pallas_call(
+    both = pl.pallas_call(
         functools.partial(body, n, cap, group),
-        out_shape=(
-            jax.ShapeDtypeStruct((tok, quarter), BF16),
-            jax.ShapeDtypeStruct((tok, quarter), BF16),
-        ),
-        in_specs=[vmem] * 9 + [hbm] * 3,
-        out_specs=(vmem, vmem),
+        out_shape=jax.ShapeDtypeStruct((2, tok, quarter), F32),
+        in_specs=[vmem] * 8 + [hbm] * 3,
+        out_specs=vmem,
         scratch_shapes=[
             pltpu.VMEM((width, hidden), BF16),
             pltpu.VMEM((width, hidden), BF16),
@@ -453,12 +482,12 @@
         tokens_b,
         norm_gain_b[None, :],
         routes.T,
-        routes,
-        route_logits,
+        route_logits.T,
         expert_gate,
         expert_up,
         expert_down,
     )
+    return both[0].astype(BF16), both[1].astype(BF16)
 
 
 def solution(mesh):

time: 81.3 us -> 67.8 us (0.83)
  Pallas kernels: 74.1 us -> 64.9 us
  local copies, waits for them, and re-layouts: 6.29 us -> 0.82 us
  other arithmetic: 0 us -> 1.29 us
    pallas_call x1, Pallas kernels: 74.1 us -> 64.9 us  [shards(): pl.pallas_call(functools.partial(body, n, cap, group), out_shape=jax.Shap...]
    unnamed x4 -> x0, local copies, waits for them, and re-layouts: 6.29 us -> none
    another operation x0 -> x1, other arithmetic: none -> 1.29 us
    convert_element_type x0 -> x1, local copies, waits for them, and re-layouts: none -> 0.82 us  [shards(): return (both[0].astype(BF16), both[1].astype(BF16))]
where the time goes in v2:
time: 67.8 us; the launch traced here: 67.6 us
  Pallas kernels  64.9 us (96%)
  other arithmetic  1.29 us (2%)
  local copies, waits for them, and re-layouts  0.82 us (1%)
    pallas_call x1, Pallas kernels, shards(): pl.pallas_call(functools.partial(body, n, cap, group), out_shape=jax.Shap...  64.9 us

profile of v2, /device:TPU:0, one launch (start us, length us, event | category | flops | bytes accessed | tf_op | source)
XLA Modules:
  0.0 67.6 jit_solution(12293749661373059507)
XLA Ops:
  0.6 64.9 %shard_map.122 = f32[2,256,512]{2,1,0:T(8,128)} custom-call(bf16[256,512]{1,0:T(8,128)(2,1)} %ta_ref.1, f32[1,512]{1,0:T(1,128)} %bitcast.10, bf16[1,512,512]{2,1,0:T(8,128)(2,1)} %pw_ref.1, f32[1,512]{1,0:T(1,128)} %bitcast.11, bf16[256,2048]{1,0:T(8,128)(2,1)} %tb_ref.1, f32[1,2048]{1,0:T(1,128)} %bitcast.9, s32[2,256]{1,0:T(2,128)} %bitcast.12, ...), custom_call_target="tpu_custom_call" | custom-call | tf_op jit(solution)/shard_map/pallas_call | solution.py:443
  65.5 1.3 %convert.4 = bf16[2,256,512]{2,1,0:T(8,128)(2,1)S(1)} convert(f32[2,256,512]{2,1,0:T(8,128)} %shard_map.122) | non-fusion elementwise | flops 262144 | bytes 1572864 | tf_op jit(solution)/shard_map/convert.1
  66.8 0.8 %slice_bitcast_fusion = (bf16[256,512]{1,0:T(8,128)(2,1)}, bf16[256,512]{1,0:T(8,128)(2,1)}) fusion(bf16[2,256,512]{2,1,0:T(8,128)(2,1)S(1)} %convert.4), kind=kLoop, calls=%fused_computation | loop fusion | bytes 1048576 | tf_op jit(solution)/shard_map/convert_element_type | solution.py:490
